TPU v7x, 32 devices: a whole 2x2x4 slice. The times are simulated.
32 devices in a mesh: sp: 8 (over z, x), tp: 4 (over y, core).
Axes of the slice: x: 2, y: 2, z: 4, core: 2. Of those that a mesh axis runs over, the one named last changes fastest.
Arguments:
- residual: bfloat16 [2048, 2048], P(('sp', 'tp')), may hold values from -6 to 6
- queries: bfloat16 [2048, 1024], P('sp', 'tp'), may hold values from -8 to 8
- key_pairs: bfloat16 [2048, 512], P('sp', 'tp'), may hold values from -8 to 8
- values: bfloat16 [2048, 512], P('sp', 'tp'), may hold values from -6 to 6
- lambdas: float32 [8], P('tp'), may hold values from 0.3 to 0.8
- head_gain: float32 [128], replicated, may hold values from 0.1 to 1.9
- out_weight: bfloat16 [1024, 2048], replicated, may hold values from -0.1875 to 0.1875
- mixer_gain: float32 [2048], replicated, may hold values from 0.1 to 1.9
- before_gain: float32 [2048], replicated, may hold values from 0.1 to 1.9
- after_gain: float32 [2048], replicated, may hold values from 0.1 to 1.9
- gate_weight: bfloat16 [2048, 5632], P('sp', 'tp'), may hold values from -0.125 to 0.125
- up_weight: bfloat16 [2048, 5632], P('sp', 'tp'), may hold values from -0.125 to 0.125
- down_weight: bfloat16 [5632, 2048], P('tp', 'sp'), may hold values from -0.078125 to 0.078125
Outputs:
- updated: bfloat16 [2048, 2048], P(('sp', 'tp'))
All inputs are finite; a program needn't handle non-finite values.
Results may differ from a plain program's by a relative error of at most 0.014.
Values may be sent and summed in bfloat16 or wider, within the bound.
A program may use at most 128 MiB of HBM per device.

v0:
```python
import math
import jax
import jax.numpy as jnp
from jax import lax
from jax.sharding import PartitionSpec as P

HEAD_DIM = 64


def row_norm(values_in, gain, epsilon):
    mean_square = jnp.mean(values_in * values_in, axis=-1, keepdims=True)
    return values_in * lax.rsqrt(mean_square + epsilon) * gain


def on_device(
    residual,
    queries,
    key_pairs,
    values,
    lambdas,
    head_gain,
    out_weight,
    mixer_gain,
    before_gain,
    after_gain,
    gate_weight,
    up_weight,
    down_weight,
):
    tokens_here = queries.shape[0]
    quarter = residual.shape[0]
    width = 2 * HEAD_DIM
    local_heads = queries.shape[1] // width
    scale = 1.0 / math.sqrt(HEAD_DIM)
    height = local_heads * tokens_here
    query_rows = jnp.transpose(
        queries.reshape(tokens_here, local_heads, 2, HEAD_DIM), (2, 1, 0, 3)
    ).reshape(2, height, HEAD_DIM)
    empty = (
        jnp.full((height,), -1e30, jnp.float32),
        jnp.zeros((height,), jnp.float32),
        jnp.zeros((height, width), jnp.float32),
    )
    state = (empty, empty)
    key_piece = lax.all_gather(key_pairs, "sp", axis=0, tiled=True)
    value_piece = lax.all_gather(values, "sp", axis=0, tiled=True)
    length = key_piece.shape[0]
    span = length
    for split_count in range(1, length + 1):
        if length % split_count == 0 and length // split_count <= 2048:
            span = length // split_count
            break
    key_blocks = key_piece.reshape(length // span, span, 2, HEAD_DIM)
    value_blocks = value_piece.reshape(length // span, span, width)

    def advance(carry, blocks_in):
        key_block, value_block = blocks_in
        renewed = []
        for which in range(2):
            running_top, running_total, running_numer = carry[which]
            score = (
                jnp.dot(
                    query_rows[which], key_block[:, which].T, preferred_element_type=jnp.float32
                )
                * scale
            )
            new_top = jnp.maximum(running_top, jnp.max(score, axis=1))
            shrink = jnp.exp(running_top - new_top)
            expo = jnp.exp(score - new_top[:, None])
            new_total = running_total * shrink + jnp.sum(expo, axis=1)
            new_numer = running_numer * shrink[:, None] + jnp.dot(
                expo.astype(jnp.bfloat16), value_block, preferred_element_type=jnp.float32
            )
            renewed.append((new_top, new_total, new_numer))
        return (tuple(renewed), None)

    state, _ = lax.scan(advance, state, (key_blocks, value_blocks))
    first_map, second_map = state
    lambda_rows = jnp.repeat(lambdas, tokens_here)[:, None]
    attended = first_map[2] / first_map[1][:, None] - lambda_rows * (
        second_map[2] / second_map[1][:, None]
    )
    normed = row_norm(attended, head_gain, 1e-05).astype(jnp.bfloat16)
    head_out = jnp.transpose(normed.reshape(local_heads, tokens_here, width), (1, 0, 2)).reshape(
        tokens_here, local_heads * width
    )
    grouped = head_out.reshape(lax.axis_size("tp"), quarter, local_heads * width)
    mixed = jnp.dot(
        lax.all_to_all(grouped, "tp", split_axis=0, concat_axis=2, tiled=True)[0],
        out_weight,
        preferred_element_type=jnp.float32,
    ).astype(jnp.bfloat16)[None][0]
    stream = residual.astype(jnp.float32) + row_norm(mixed.astype(jnp.float32), mixer_gain, 1e-06)
    normed_in = row_norm(stream, before_gain, 1e-06).astype(jnp.bfloat16)
    gathered = lax.all_gather(normed_in, "tp", axis=0, tiled=True)
    empty_hidden = jnp.zeros((gathered.shape[0], gate_weight.shape[1]), jnp.float32)
    pieces = (
        lax.all_gather(gate_weight, "sp", axis=0, tiled=True),
        lax.all_gather(up_weight, "sp", axis=0, tiled=True),
    )
    columns = lax.slice_in_dim(gathered, 0, pieces[0].shape[0], axis=1)
    gate_part = jnp.dot(columns, pieces[0], preferred_element_type=jnp.float32)
    up_part = jnp.dot(columns, pieces[1], preferred_element_type=jnp.float32)
    gate = empty_hidden + gate_part
    up = empty_hidden + up_part
    down_whole = lax.all_gather(down_weight, "sp", axis=1, tiled=True)
    hidden = (jax.nn.silu(gate) * up).astype(jnp.bfloat16)
    picked = lax.slice_in_dim(hidden, 0, lax.axis_size("tp") * quarter, axis=0)
    channel = lax.psum_scatter(
        jnp.dot(picked, down_whole, preferred_element_type=jnp.float32).astype(jnp.bfloat16),
        "tp",
        scatter_dimension=0,
        tiled=True,
    )
    updated = stream + 0.5 * row_norm(channel.astype(jnp.float32), after_gain, 1e-06)
    return updated.astype(jnp.bfloat16)


def solution(mesh):
    return jax.shard_map(
        on_device,
        mesh=mesh,
        in_specs=(
            P(("sp", "tp"), None),
            P("sp", "tp"),
            P("sp", "tp"),
            P("sp", "tp"),
            P("tp"),
            P(),
            P(),
            P(),
            P(),
            P(),
            P("sp", "tp"),
            P("sp", "tp"),
            P("tp", "sp"),
        ),
        out_specs=P(("sp", "tp"), None),
        check_vma=False,
    )
```

profile of v0, /device:TPU:0, one launch (start us, length us, event | category | flops | bytes accessed | tf_op | source)
XLA Modules:
  0.0 430.2 jit_solution(3633528644462433819)
XLA Ops:
  6.5 0.9 copy.16
  7.5 33.0 %all_gather.18 = bf16[2048,128]{0,1:T(8,128)(2,1)S(1)} all-gather(bf16[256,128]{0,1:T(8,128)(2,1)S(1)} %copy.16), channel_id=1, replica_groups=mesh['sp'=8,'tp'=4] {'sp'}, dimensions={0}, use_global_device_ids=true | all-gather | bytes 589824 | tf_op jit(solution)/shard_map/all_gather | solution.py:45
  40.5 1.0 copy.14
  41.7 0.8 multiply_reduce_fusion.1
  42.5 0.8 fusion
  43.3 31.3 %all_gather.19 = bf16[2048,128]{1,0:T(8,128)(2,1)S(1)} all-gather(bf16[256,128]{1,0:T(8,128)(2,1)S(1)} %copy-done.3), channel_id=1, replica_groups=mesh['sp'=8,'tp'=4] {'sp'}, dimensions={0}, use_global_device_ids=true | all-gather | bytes 589824 | tf_op jit(solution)/shard_map/all_gather | solution.py:46
  74.7 0.8 multiply_reduce_fusion
  75.5 0.8 fusion.2
  76.5 0.9 fusion.29
  77.4 1.5 multiply_reduce_fusion.4
  79.3 7.2 %all_to_all.15 = bf16[4,64,256]{2,1,0:T(8,128)(2,1)S(1)} all-to-all(bf16[4,64,256]{2,1,0:T(8,128)(2,1)S(1)} %reshape_reshape.3), channel_id=1, replica_groups=mesh['sp'=8,'tp'=4] {'tp'}, dimensions={0} | all-to-all | bytes 262144 | tf_op jit(solution)/shard_map/all_to_all | solution.py:89
  86.6 3.1 multiply_reduce_fusion.3
  90.1 0.9 multiply_convert_fusion
  91.0 0.7 all-gather.7.cloned.1.call-update
  91.8 0.7 all-gather.11.cloned.1.call-update
  93.1 15.0 %all-gather.5.cloned.1.call-done = bf16[256,2048]{1,0:T(8,128)(2,1)} async-done(((bf16[64,2048]{1,0:T(8,128)(2,1)}), bf16[256,2048]{1,0:T(8,128)(2,1)}) %all-gather.5.cloned.1.call-update) | async-done | bytes 1048592 | tf_op jit(solution)/shard_map/all_gather | solution.py:95
  108.1 94.5 %all-gather.7.cloned.1.call-done = bf16[2048,1408]{1,0:T(8,128)(2,1)} async-done(((bf16[256,1408]{1,0:T(8,128)(2,1)}), bf16[2048,1408]{1,0:T(8,128)(2,1)}) %all-gather.7.cloned.1.call-update) | async-done | bytes 5767184 | tf_op jit(solution)/shard_map/all_gather | solution.py:98
  202.6 4.8 %fusion.45 = f32[256,1408]{1,0:T(8,128)S(1)} fusion(bf16[256,2048]{1,0:T(8,128)(2,1)} %all-gather.5.cloned.1.call-done, bf16[2048,1408]{1,0:T(8,128)(2,1)} %all-gather.7.cloned.1.call-done), kind=kOutput, calls=%fused_computation.58 | convolution fusion | flops 1476395008 | bytes 8257536 | tf_op jit(solution)/shard_map/dot_general | solution.py:102
  207.4 88.6 %all-gather.11.cloned.1.call-done = bf16[1408,2048]{1,0:T(8,128)(2,1)} async-done(((bf16[1408,256]{1,0:T(8,128)(2,1)}), bf16[1408,2048]{1,0:T(8,128)(2,1)}) %all-gather.11.cloned.1.call-update) | async-done | bytes 5767184 | tf_op jit(solution)/shard_map/all_gather | solution.py:106
  296.0 92.6 %all-gather.9.cloned.1.call-done = bf16[2048,1408]{1,0:T(8,128)(2,1)} async-done(((bf16[256,1408]{1,0:T(8,128)(2,1)}), bf16[2048,1408]{1,0:T(8,128)(2,1)}) %all-gather.9.cloned.1.call-update) | async-done | bytes 5767184 | tf_op jit(solution)/shard_map/all_gather | solution.py:99
  388.6 8.9 %convolution_convert_fusion = bf16[256,2048]{1,0:T(8,128)(2,1)} fusion(bf16[1408,2048]{1,0:T(8,128)(2,1)} %all-gather.11.cloned.1.call-done, bf16[256,2048]{1,0:T(8,128)(2,1)S(1)} %copy-done.7, bf16[2048,1408]{1,0:T(8,128)(2,1)} %all-gather.9.cloned.1.call-done, f32[256,1408]{1,0:T(8,128)S(1)} %fusion.45), kind=kOutput, calls=%fused_computation.10 | convolution fusion | flops 2955476992 | bytes 15073280 | tf_op jit(solution)/shard_map/dot_general | solution.py:110
  397.5 23.1 %reduce-scatter.2.cloned.1.call-done = bf16[64,2048]{1,0:T(8,128)(2,1)} async-done(((bf16[256,2048]{1,0:T(8,128)(2,1)}), bf16[64,2048]{1,0:T(8,128)(2,1)}) %reduce-scatter.2.cloned.1.call-update) | async-done | bytes 262160 | tf_op jit(solution)/shard_map/reduce_scatter | solution.py:109
  420.6 1.1 fusion.32
  421.7 1.9 fusion.36
  (45 shorter events, 1.8 us)
Async XLA Ops:
  6.5 69.8 %copy-start = (f32[2]{0:T(128)S(1)}, f32[2]{0:T(128)}, u32[]{:S(2)}) copy-start(f32[2]{0:T(128)} %param.17) | copy-start | bytes 28
  6.5 101.6 %all-gather.5.cloned.1.call-start = ((), (), s32[]{:S(2)}) async-start(), calls=%async_computation.2 | async-start | bytes 1310720 | tf_op jit(solution)/shard_map/all_gather | solution.py:95
  41.7 1.7 copy-start.3
  77.3 1.6 copy-start.6
  78.8 10.9 %copy-start.1 = (bf16[64,2048]{1,0:T(8,128)(2,1)S(1)}, bf16[64,2048]{1,0:T(8,128)(2,1)}, u32[]{:S(2)}) copy-start(bf16[64,2048]{1,0:T(8,128)(2,1)} %param.13) | copy-start | bytes 786436
  78.9 10.9 %copy-start.2 = (f32[2048]{0:T(1024)S(1)}, f32[2048]{0:T(1024)}, u32[]{:S(2)}) copy-start(f32[2048]{0:T(1024)} %param.20) | copy-start | bytes 24580
  78.9 11.2 %copy-start.4 = (f32[2048]{0:T(1024)S(1)}, f32[2048]{0:T(1024)}, u32[]{:S(2)}) copy-start(f32[2048]{0:T(1024)} %param.21) | copy-start | bytes 24580
  91.0 111.6 %all-gather.7.cloned.1.call-start = ((), (), s32[]{:S(2)}) async-start(), calls=%async_computation.3 | async-start | bytes 6488064 | tf_op jit(solution)/shard_map/all_gather | solution.py:98
  91.8 204.3 %all-gather.11.cloned.1.call-start = ((), (), s32[]{:S(2)}) async-start(), calls=%async_computation.5 | async-start | bytes 6488064 | tf_op jit(solution)/shard_map/all_gather | solution.py:106
  92.5 296.1 %all-gather.9.cloned.1.call-start = ((), (), s32[]{:S(2)}) async-start(), calls=%async_computation.4 | async-start | bytes 6488064 | tf_op jit(solution)/shard_map/all_gather | solution.py:99
  93.1 327.5 %reduce-scatter.2.cloned.1.call-start = ((), (), s32[]{:S(2)}) async-start(), calls=%async_computation.6 | async-start | bytes 1310720 | tf_op jit(solution)/shard_map/reduce_scatter | solution.py:109
  108.1 280.5 %copy-start.7 = (bf16[256,2048]{1,0:T(8,128)(2,1)S(1)}, bf16[256,2048]{1,0:T(8,128)(2,1)}, u32[]{:S(2)}) copy-start(bf16[256,2048]{1,0:T(8,128)(2,1)} %all-gather.5.cloned.1.call-done) | copy-start | bytes 3145732
  207.4 214.3 %copy-start.5 = (f32[2048]{0:T(1024)S(1)}, f32[2048]{0:T(1024)}, u32[]{:S(2)}) copy-start(f32[2048]{0:T(1024)} %param.22) | copy-start | bytes 24580
Sparse Core Ops, SparseCore 0:
  91.1 16.9 all-gather.4
  110.3 92.2 all-gather.6
  204.7 91.2 all-gather.10
  298.1 90.4 all-gather.8
  397.6 22.9 reduce-scatter.1
where the time goes:
time: 431 us; the launch traced here: 430 us
  waiting for transfers between devices  316 us (73%)
  blocking collectives  71.5 us (17%)
  matrix products  20.8 us (5%)
  between operations  13.4 us (3%)
  other arithmetic  6.02 us (1%)
    all_gather x1, waiting for transfers between devices, on_device(): lax.all_gather(gate_weight, 'sp', axis=0, tiled=True)  94.5 us
    all_gather x1, waiting for transfers between devices, on_device(): lax.all_gather(up_weight, 'sp', axis=0, tiled=True)  92.6 us
    all_gather x1, waiting for transfers between devices, on_device(): down_whole = lax.all_gather(down_weight, 'sp', axis=1, tiled=True)  88.6 us
    all_gather x1, blocking collectives, on_device(): key_piece = lax.all_gather(key_pairs, 'sp', axis=0, tiled=True)  33 us
    all_gather x1, blocking collectives, on_device(): value_piece = lax.all_gather(values, 'sp', axis=0, tiled=True)  31.3 us
    reduce_scatter x1, waiting for transfers between devices, on_device(): lax.psum_scatter(jnp.dot(picked, down_whole, preferred_element_type=jnp.f...  23.1 us
    all_gather x1, waiting for transfers between devices, on_device(): gathered = lax.all_gather(normed_in, 'tp', axis=0, tiled=True)  15 us
    dot_general x1, matrix products, on_device(): jnp.dot(picked, down_whole, preferred_element_type=jnp.float32)  8.9 us
  transfers between devices with their start and end apart: 5, of which 5 were waited for; matrix products, arithmetic and copies ran while one was open for 1% of the time, Pallas kernels for 0%

commit v1 on v0

--- a/solution.py
+++ b/solution.py
@@ -42,8 +42,11 @@
         jnp.zeros((height, width), jnp.float32),
     )
     state = (empty, empty)
-    key_piece = lax.all_gather(key_pairs, "sp", axis=0, tiled=True)
-    value_piece = lax.all_gather(values, "sp", axis=0, tiled=True)
+    key_piece, value_piece = jnp.split(
+        lax.all_gather(jnp.concatenate([key_pairs, values], axis=1), "sp", axis=0, tiled=True),
+        [key_pairs.shape[1]],
+        axis=1,
+    )
     length = key_piece.shape[0]
     span = length
     for split_count in range(1, length + 1):

time: 431 us -> 407 us (0.944)
  blocking collectives: 71.5 us -> 7.26 us
  waiting for transfers between devices: 316 us -> 354 us
    all_gather x2 -> x0, blocking collectives: 64.3 us -> none  [the longest x1 33 us: on_device(): key_piece = lax.all_gather(key_pairs, 'sp', axis=0, tiled=True)]
    all_gather x0 -> x1, waiting for transfers between devices: none -> 41 us  [on_device(): lax.all_gather(jnp.concatenate([key_pairs, values], axis=1), 'sp', axis=0...]
    all_gather x1, waiting for transfers between devices: 92.6 us -> 87.8 us  [on_device(): lax.all_gather(up_weight, 'sp', axis=0, tiled=True)]
    all_gather x1, waiting for transfers between devices: 88.6 us -> 93.2 us  [on_device(): down_whole = lax.all_gather(down_weight, 'sp', axis=1, tiled=True)]
  transfers between devices with their start and end apart: 5 -> 6, of which waited for: 5 -> 6; matrix products, arithmetic and copies ran while one was open for 1% -> 1% of each run, Pallas kernels for 0% -> 0%
where the time goes in v1:
time: 407 us
  waiting for transfers between devices  354 us (87%)
  matrix products  20.4 us (5%)
  between operations  13.7 us (3%)
  blocking collectives  7.26 us (2%)
  other arithmetic  6.53 us (2%)
  local copies, waits for them, and re-layouts  4.6 us (1%)
    all_gather x1, waiting for transfers between devices, on_device(): lax.all_gather(gate_weight, 'sp', axis=0, tiled=True)  94.5 us
    all_gather x1, waiting for transfers between devices, on_device(): down_whole = lax.all_gather(down_weight, 'sp', axis=1, tiled=True)  93.2 us
    all_gather x1, waiting for transfers between devices, on_device(): lax.all_gather(up_weight, 'sp', axis=0, tiled=True)  87.8 us
    all_gather x1, waiting for transfers between devices, on_device(): lax.all_gather(jnp.concatenate([key_pairs, values], axis=1), 'sp', axis=0...  41 us
    reduce_scatter x1, waiting for transfers between devices, on_device(): lax.psum_scatter(jnp.dot(picked, down_whole, preferred_element_type=jnp.f...  23.1 us
    all_gather x1, waiting for transfers between devices, on_device(): gathered = lax.all_gather(normed_in, 'tp', axis=0, tiled=True)  12.9 us
    dot_general x1, matrix products, on_device(): jnp.dot(picked, down_whole, preferred_element_type=jnp.float32)  8.92 us
  transfers between devices with their start and end apart: 6, of which 6 were waited for; matrix products, arithmetic and copies ran while one was open for 1% of the time, Pallas kernels for 0%

profile of v1, /device:TPU:0, one launch (start us, length us, event | category | flops | bytes accessed | tf_op | source)
XLA Modules:
  0.0 407.1 jit_solution(8910368274869061140)
XLA Ops:
  6.5 0.9 copy.14
  7.5 0.9 copy.15
  9.2 1.0 copy.16
  10.5 41.0 %all-gather.6.cloned.1.call-done = bf16[2048,256]{0,1:T(8,128)(2,1)} async-done(((bf16[256,256]{0,1:T(8,128)(2,1)}), bf16[2048,256]{0,1:T(8,128)(2,1)}) %all-gather.6.cloned.1.call-update) | async-done | bytes 1048592 | tf_op jit(solution)/shard_map/all_gather | solution.py:46
  51.5 1.1 split.8
  52.6 0.7 multiply_reduce_fusion.1
  53.4 0.8 fusion
  54.1 0.7 multiply_reduce_fusion
  54.9 0.8 fusion.2
  55.7 0.9 fusion.29
  56.6 1.1 multiply_reduce_fusion.4
  58.2 7.3 %all_to_all.15 = bf16[4,64,256]{2,1,0:T(8,128)(2,1)S(1)} all-to-all(bf16[4,64,256]{2,1,0:T(8,128)(2,1)S(1)} %reshape_reshape.3), channel_id=1, replica_groups=mesh['sp'=8,'tp'=4] {'tp'}, dimensions={0} | all-to-all | bytes 262144 | tf_op jit(solution)/shard_map/all_to_all | solution.py:92
  65.6 3.1 multiply_reduce_fusion.3
  69.0 0.9 multiply_convert_fusion
  70.0 0.7 all-gather.10.cloned.1.call-update
  71.9 12.9 %all-gather.8.cloned.1.call-done = bf16[256,2048]{1,0:T(8,128)(2,1)} async-done(((bf16[64,2048]{1,0:T(8,128)(2,1)}), bf16[256,2048]{1,0:T(8,128)(2,1)}) %all-gather.8.cloned.1.call-update) | async-done | bytes 1048592 | tf_op jit(solution)/shard_map/all_gather | solution.py:98
  84.8 94.5 %all-gather.10.cloned.1.call-done = bf16[2048,1408]{1,0:T(8,128)(2,1)} async-done(((bf16[256,1408]{1,0:T(8,128)(2,1)}), bf16[2048,1408]{1,0:T(8,128)(2,1)}) %all-gather.10.cloned.1.call-update) | async-done | bytes 5767184 | tf_op jit(solution)/shard_map/all_gather | solution.py:101
  179.3 4.8 %fusion.47 = f32[256,1408]{1,0:T(8,128)S(1)} fusion(bf16[256,2048]{1,0:T(8,128)(2,1)} %all-gather.8.cloned.1.call-done, bf16[2048,1408]{1,0:T(8,128)(2,1)} %all-gather.10.cloned.1.call-done), kind=kOutput, calls=%fused_computation.61 | convolution fusion | flops 1476395008 | bytes 8257536 | tf_op jit(solution)/shard_map/dot_general | solution.py:105
  184.1 87.8 %all-gather.12.cloned.1.call-done = bf16[2048,1408]{1,0:T(8,128)(2,1)} async-done(((bf16[256,1408]{1,0:T(8,128)(2,1)}), bf16[2048,1408]{1,0:T(8,128)(2,1)}) %all-gather.12.cloned.1.call-update) | async-done | bytes 5767184 | tf_op jit(solution)/shard_map/all_gather | solution.py:102
  271.9 93.2 %all-gather.14.cloned.1.call-done = bf16[1408,2048]{1,0:T(8,128)(2,1)} async-done(((bf16[1408,256]{1,0:T(8,128)(2,1)}), bf16[1408,2048]{1,0:T(8,128)(2,1)}) %all-gather.14.cloned.1.call-update) | async-done | bytes 5767184 | tf_op jit(solution)/shard_map/all_gather | solution.py:109
  365.1 8.9 %convolution_convert_fusion = bf16[256,2048]{1,0:T(8,128)(2,1)} fusion(bf16[1408,2048]{1,0:T(8,128)(2,1)} %all-gather.14.cloned.1.call-done, bf16[256,2048]{1,0:T(8,128)(2,1)S(1)} %copy-done.7, bf16[2048,1408]{1,0:T(8,128)(2,1)} %all-gather.12.cloned.1.call-done, f32[256,1408]{1,0:T(8,128)S(1)} %fusion.47), kind=kOutput, calls=%fused_computation.10 | convolution fusion | flops 2955476992 | bytes 15073280 | tf_op jit(solution)/shard_map/dot_general | solution.py:113
  374.1 23.1 %reduce-scatter.2.cloned.1.call-done = bf16[64,2048]{1,0:T(8,128)(2,1)} async-done(((bf16[256,2048]{1,0:T(8,128)(2,1)}), bf16[64,2048]{1,0:T(8,128)(2,1)}) %reduce-scatter.2.cloned.1.call-update) | async-done | bytes 262160 | tf_op jit(solution)/shard_map/reduce_scatter | solution.py:112
  397.2 1.1 fusion.32
  398.3 1.9 fusion.36
  (49 shorter events, 3.1 us)
Async XLA Ops:
  6.5 3.9 copy-start
  6.5 45.0 %all-gather.6.cloned.1.call-start = ((), (), s32[]{:S(2)}) async-start(), calls=%async_computation.2 | async-start | bytes 1179648 | tf_op jit(solution)/shard_map/all_gather | solution.py:46
  9.1 75.7 %all-gather.8.cloned.1.call-start = ((), (), s32[]{:S(2)}) async-start(), calls=%async_computation.3 | async-start | bytes 1310720 | tf_op jit(solution)/shard_map/all_gather | solution.py:98
  54.1 1.5 copy-start.2
  56.6 1.2 copy-start.6
  57.7 11.0 %copy-start.1 = (bf16[64,2048]{1,0:T(8,128)(2,1)S(1)}, bf16[64,2048]{1,0:T(8,128)(2,1)}, u32[]{:S(2)}) copy-start(bf16[64,2048]{1,0:T(8,128)(2,1)} %param.13) | copy-start | bytes 786436
  57.8 11.0 %copy-start.3 = (f32[2048]{0:T(1024)S(1)}, f32[2048]{0:T(1024)}, u32[]{:S(2)}) copy-start(f32[2048]{0:T(1024)} %param.20) | copy-start | bytes 24580
  57.8 11.3 %copy-start.4 = (f32[2048]{0:T(1024)S(1)}, f32[2048]{0:T(1024)}, u32[]{:S(2)}) copy-start(f32[2048]{0:T(1024)} %param.21) | copy-start | bytes 24580
  70.0 109.4 %all-gather.10.cloned.1.call-start = ((), (), s32[]{:S(2)}) async-start(), calls=%async_computation.4 | async-start | bytes 6488064 | tf_op jit(solution)/shard_map/all_gather | solution.py:101
  70.7 201.2 %all-gather.12.cloned.1.call-start = ((), (), s32[]{:S(2)}) async-start(), calls=%async_computation.5 | async-start | bytes 6488064 | tf_op jit(solution)/shard_map/all_gather | solution.py:102
  71.3 293.9 %all-gather.14.cloned.1.call-start = ((), (), s32[]{:S(2)}) async-start(), calls=%async_computation.6 | async-start | bytes 6488064 | tf_op jit(solution)/shard_map/all_gather | solution.py:109
  71.9 325.3 %reduce-scatter.2.cloned.1.call-start = ((), (), s32[]{:S(2)}) async-start(), calls=%async_computation.7 | async-start | bytes 1310720 | tf_op jit(solution)/shard_map/reduce_scatter | solution.py:112
  84.8 280.3 %copy-start.7 = (bf16[256,2048]{1,0:T(8,128)(2,1)S(1)}, bf16[256,2048]{1,0:T(8,128)(2,1)}, u32[]{:S(2)}) copy-start(bf16[256,2048]{1,0:T(8,128)(2,1)} %all-gather.8.cloned.1.call-done) | copy-start | bytes 3145732
  184.1 214.2 %copy-start.5 = (f32[2048]{0:T(1024)S(1)}, f32[2048]{0:T(1024)}, u32[]{:S(2)}) copy-start(f32[2048]{0:T(1024)} %param.22) | copy-start | bytes 24580
Sparse Core Ops, SparseCore 0:
  9.4 42.1 all-gather.5
  70.1 14.6 all-gather.7
  87.0 92.2 all-gather.9
  181.4 90.4 all-gather.11
  273.8 91.2 all-gather.13
  374.2 22.9 reduce-scatter.1
